TPU v7x, 256 devices: a 8x8x2 block of a 8x8x16 slice. The times are simulated.
256 devices in a mesh: grp: 2 (over z), ep: 16 (over y, core), tp: 8 (over x).
Axes of the slice: x: 8, y: 8, z: 2, core: 2. Of those that a mesh axis runs over, the one named last changes fastest.
The devices are a block of a 8x8x16 slice.
Arguments:
- mixer_in: bfloat16 [32768, 2048], P(('grp', 'ep', 'tp')), parts along dimension 0, may hold values from -600 to 600
- mixer_gain: float32 [2048], replicated, may hold values from 0.1 to 1.9
- w_query: bfloat16 [2048, 1024], P(None, 'tp'), may hold values from -6 to 6
- w_key: bfloat16 [2048, 512], P(None, 'tp'), may hold values from -0.1875 to 0.1875
- w_value: bfloat16 [2048, 512], P(None, 'tp'), may hold values from -0.25 to 0.25
- sink_logit: float32 [16], P('tp'), may hold values from 3 to 9
- moe_in: bfloat16 [32768, 2048], P(('grp', 'ep', 'tp')), parts along dimension 0, may hold values from -600 to 600
- moe_gain: float32 [2048], replicated, may hold values from 0.1 to 1.9
- router: bfloat16 [2048, 128], replicated, may hold values from -0.25 to 0.25
- routes: int32 [32768, 4], P(('grp', 'ep', 'tp')), parts along dimension 0, may hold values from 0 to 127, all different within a row; in each aligned block of 128 rows (0 to 127, 128 to 255, ...) at most 6 rows name the same one
- expert_gate: bfloat16 [128, 2048, 512], P(('ep', 'tp')), may hold values from -0.125 to 0.125
- expert_up: bfloat16 [128, 2048, 512], P(('ep', 'tp')), may hold values from -0.125 to 0.125
- expert_down: bfloat16 [128, 512, 2048], P(('ep', 'tp')), may hold values from -0.25 to 0.25
- shared_gate: bfloat16 [2048, 512], P(None, 'tp'), may hold values from -0.125 to 0.125
- shared_up: bfloat16 [2048, 512], P(None, 'tp'), may hold values from -0.125 to 0.125
- shared_down: bfloat16 [512, 2048], P('tp'), may hold values from -0.25 to 0.25
Outputs:
- mixed: bfloat16 [32768, 1024], P(('grp', 'ep'), 'tp'), parts along dimension 0
- moe_out: bfloat16 [32768, 2048], P(('grp', 'ep', 'tp')), parts along dimension 0
There are 2 independent parts, one for each index of `grp`. A program takes and returns all parts, laid end to end along the dimension named above; an argument that names none is the same for every part. Nothing has to cross between parts.
Inputs may be any that keep to these rules, and one draw needn't show every extreme that they name: `routes`: each row names 4 different experts. Within the rows of one device (aligned blocks of 128 rows) no expert is named by more than 6 rows, a bound that some block reaches.
All inputs are finite; a program needn't handle non-finite values.
Results may differ from a plain program's by a relative error of at most 0.012.
Values may be sent and summed in bfloat16 or wider, within the bound.
No kernel may reach another device: no remote copies, remote signals or barrier semaphores. Data moves between devices by JAX's collectives and lax.ppermute only.
A program may use at most 128 MiB of HBM per device.

v0:
```python
import jax
import jax.numpy as jnp
from jax import lax
from jax.sharding import PartitionSpec as P

HEAD_DIM = 64
WINDOW = 128


EPS = 1e-06
THETA = 10000.0
ROUTED_SCALE = 2.5


def turned_gather(arrays, axis, dims):
    turned = [jnp.moveaxis(a, dim, 0) for a, dim in zip(arrays, dims)]
    both = jnp.concatenate([t.reshape(len(t), -1) for t in turned], axis=1)
    whole, at, done = (lax.all_gather(both, axis, axis=0, tiled=True), 0, [])
    for t, dim in zip(turned, dims):
        piece = whole[:, at : at + t[0].size].reshape(-1, *t.shape[1:])
        done.append(jnp.moveaxis(piece, 0, dim))
        at += t[0].size
    return tuple(done)


def extended(block, sides, width):
    for axis, dim in sides:
        count = lax.axis_size(axis)
        forward = [(i, i + 1) for i in range(count - 1)]
        backward = [(target, source) for source, target in forward]
        low = lax.ppermute(
            lax.slice_in_dim(block, block.shape[dim] - width, None, axis=dim), axis, forward
        )
        high = lax.ppermute(lax.slice_in_dim(block, 0, width, axis=dim), axis, backward)
        block = jnp.concatenate([low, block, high], axis=dim)
    return block


def rms_rows(row_block, gain_vector):
    values = row_block.astype(jnp.float32)
    factor = lax.rsqrt(jnp.mean(values * values, axis=-1, keepdims=True) + EPS)
    return (values * factor * gain_vector).astype(jnp.bfloat16)


def rotate(head_rows, positions):
    half_width = head_rows.shape[-1] // 2
    inverse = THETA ** (-(jnp.arange(half_width, dtype=jnp.float32) * 2.0) / head_rows.shape[-1])
    angles = positions.astype(jnp.float32)[:, None] * inverse[None, :]
    cosine_table = jnp.cos(angles)[:, None, :]
    sine_table = jnp.sin(angles)[:, None, :]
    first_half = head_rows[..., :half_width]
    second_half = head_rows[..., half_width:]
    return jnp.concatenate(
        [
            first_half * cosine_table - second_half * sine_table,
            second_half * cosine_table + first_half * sine_table,
        ],
        axis=-1,
    )


def attend(query_rows, stacked, sink_logit, offset, seq_length):
    span_rows, head_count, head_width = query_rows.shape
    kv_local = stacked.shape[1] // (2 * head_width)
    group_size = head_count // kv_local
    key_table = stacked[:, : kv_local * head_width].reshape(-1, kv_local, head_width)
    value_table = stacked[:, kv_local * head_width :].reshape(-1, kv_local, head_width)
    block_rows = 512
    grouped = query_rows.reshape(span_rows, kv_local, group_size, head_width)
    row_ids = jnp.arange(block_rows, dtype=jnp.int32)[:, None]
    col_ids = jnp.arange(block_rows + 2 * WINDOW, dtype=jnp.int32)[None, :]
    sink_table = sink_logit.reshape(kv_local, group_size)[:, :, None, None]

    def one_block(block_index):
        block_start = block_index * block_rows
        query_block = lax.dynamic_slice_in_dim(grouped, block_start, block_rows, 0)
        key_block = lax.dynamic_slice_in_dim(key_table, block_start, block_rows + 2 * WINDOW, 0)
        value_block = lax.dynamic_slice_in_dim(value_table, block_start, block_rows + 2 * WINDOW, 0)
        scores = jnp.einsum(
            "qkgd,ckd->kgqc", query_block, key_block, preferred_element_type=jnp.float32
        ) * head_width ** (-0.5)
        key_pos = offset + block_start - WINDOW + col_ids
        query_pos = offset + block_start + row_ids
        in_window = (
            (jnp.abs(key_pos - query_pos) <= WINDOW) & (key_pos >= 0) & (key_pos < seq_length)
        )
        scores = jnp.where(in_window[None, None], scores, -jnp.inf)
        row_max = jnp.maximum(jnp.max(scores, axis=-1, keepdims=True), sink_table)
        weights = jnp.exp(scores - row_max)
        denominator = jnp.sum(weights, axis=-1, keepdims=True) + jnp.exp(sink_table - row_max)
        probability = (weights / denominator).astype(jnp.bfloat16)
        output = jnp.einsum(
            "kgqc,ckd->qkgd", probability, value_block, preferred_element_type=jnp.float32
        )
        return output.reshape(block_rows, head_count * head_width).astype(jnp.bfloat16)

    blocks_out = lax.map(one_block, jnp.arange(span_rows // block_rows, dtype=jnp.int32))
    return blocks_out.reshape(span_rows, head_count * head_width)


def body(
    mixer_in,
    mixer_gain,
    w_query,
    w_key,
    w_value,
    sink_logit,
    moe_in,
    moe_gain,
    router,
    routes,
    expert_gate,
    expert_up,
    expert_down,
    shared_gate,
    shared_up,
    shared_down,
):
    normed_first = rms_rows(mixer_in, mixer_gain)
    normed_second = rms_rows(moe_in, moe_gain)
    query_cols = w_query.shape[1]
    key_cols = w_key.shape[1]
    joined = jnp.concatenate([w_query, w_key, w_value], axis=1)
    projected = jnp.dot(
        lax.all_gather(normed_first, "tp", axis=0, tiled=True),
        joined,
        preferred_element_type=jnp.float32,
    )
    full_gate, full_up, full_down = turned_gather(
        (shared_gate, shared_up, shared_down), "tp", (1, 1, 0)
    )
    hidden = (
        jax.nn.silu(jnp.dot(normed_second, full_gate, preferred_element_type=jnp.float32))
        * jnp.dot(normed_second, full_up, preferred_element_type=jnp.float32)
    ).astype(jnp.bfloat16)
    shared = jnp.dot(hidden, full_down, preferred_element_type=jnp.float32)
    span_rows = projected.shape[0]
    offset = lax.axis_index("ep") * span_rows
    seq_length = span_rows * lax.axis_size("ep")
    positions = offset + jnp.arange(span_rows, dtype=jnp.int32)
    query_rows = rotate(
        projected[:, :query_cols].reshape(span_rows, -1, HEAD_DIM), positions
    ).astype(jnp.bfloat16)
    key_rows = rotate(
        projected[:, query_cols : query_cols + key_cols].reshape(span_rows, -1, HEAD_DIM), positions
    ).astype(jnp.bfloat16)
    value_rows = projected[:, query_cols + key_cols :].astype(jnp.bfloat16)
    stacked = jnp.concatenate([key_rows.reshape(span_rows, key_cols), value_rows], axis=1)
    padded = extended(stacked, (("ep", 0),), WINDOW)
    mixed = attend(query_rows, padded, sink_logit, offset, seq_length)
    tokens = normed_second.shape[0]
    top_count = routes.shape[1]
    experts = router.shape[1]
    capacity = 3 * top_count * tokens // (2 * experts)
    affinity = jax.nn.sigmoid(jnp.dot(normed_second, router, preferred_element_type=jnp.float32))
    hit_table = routes[:, :, None] == jnp.arange(experts, dtype=jnp.int32)[None, None, :]
    chosen = jnp.sum(jnp.where(hit_table, affinity[:, None, :], 0.0), axis=-1)
    route_weight = ROUTED_SCALE * chosen / jnp.sum(chosen, axis=-1, keepdims=True)
    flat_hits = hit_table.reshape(tokens * top_count, experts).astype(jnp.int32)
    slot_index = jnp.sum((jnp.cumsum(flat_hits, axis=0) - 1) * flat_hits, axis=-1)
    target = routes.reshape(-1) * capacity + slot_index
    source = jnp.arange(tokens * top_count, dtype=jnp.int32) // top_count
    outgoing = (
        jnp.zeros((experts * capacity, normed_second.shape[1]), jnp.bfloat16)
        .at[target]
        .set(normed_second[source])
    )
    outgoing = outgoing.reshape(experts, capacity, -1)
    row_block = lax.all_to_all(outgoing, ("ep", "tp"), split_axis=0, concat_axis=0, tiled=True)
    row_shape = row_block.shape
    flat_rows = row_block.reshape(-1, row_shape[-1])
    hidden_rows = (
        jax.nn.silu(jnp.dot(flat_rows, expert_gate[0], preferred_element_type=jnp.float32))
        * jnp.dot(flat_rows, expert_up[0], preferred_element_type=jnp.float32)
    ).astype(jnp.bfloat16)
    returned = lax.all_to_all(
        jnp.dot(hidden_rows, expert_down[0], preferred_element_type=jnp.float32)
        .astype(jnp.bfloat16)
        .reshape(row_shape),
        ("ep", "tp"),
        split_axis=0,
        concat_axis=0,
        tiled=True,
    )
    picked = returned.reshape(experts * capacity, -1)[target].reshape(tokens, top_count, -1)
    routed = jnp.sum(picked.astype(jnp.float32) * route_weight[:, :, None], axis=1)
    moe_out = (routed + shared).astype(jnp.bfloat16)
    return (mixed, moe_out)


def solution(mesh):
    return jax.shard_map(
        body,
        mesh=mesh,
        in_specs=(
            P(("grp", "ep", "tp"), None),
            P(),
            P(None, "tp"),
            P(None, "tp"),
            P(None, "tp"),
            P("tp"),
            P(("grp", "ep", "tp"), None),
            P(),
            P(),
            P(("grp", "ep", "tp"), None),
            P(("ep", "tp"), None, None),
            P(("ep", "tp"), None, None),
            P(("ep", "tp"), None, None),
            P(None, "tp"),
            P(None, "tp"),
            P("tp", None),
        ),
        out_specs=(P(("grp", "ep"), "tp"), P(("grp", "ep", "tp"), None)),
        check_vma=False,
    )
```

profile of v0, /device:TPU:513, one launch (start us, length us, event | category | flops | bytes accessed | tf_op | source)
XLA Modules:
  0.0 361.7 jit_solution(15444684398977455137)
XLA Ops:
  8.7 2.0 fusion.54
  13.2 12.6 %scatter_custom_fusion = bf16[768,2048]{1,0:T(8,128)(2,1)} fusion(s32[512]{0:T(512)S(1)} %bitcast.124, bf16[128,2048]{1,0:T(8,128)(2,1)S(1)} %fusion.57, s32[1024]{0:T(1024)S(1)} %pad_clamp_fusion.1, bf16[]{:T(256)} %constant.110.clone.1), kind=kCustom, calls=%fused_computation.49 | custom fusion | bytes 3145730 | tf_op jit(solution)/shard_map/scatter | solution.py:166
  25.7 6.2 %reshape.556 = bf16[128,6,2048]{2,1,0:T(8,128)(2,1)} reshape(bf16[768,2048]{1,0:T(8,128)(2,1)} %scatter_custom_fusion) | data formatting | bytes 6291456 | tf_op jit(solution)/shard_map/reshape | solution.py:168
  32.0 28.5 %all-to-all-start = ((bf16[128,6,2048]{2,1,0:T(8,128)(2,1)}), bf16[128,6,2048]{2,1,0:T(8,128)(2,1)}, u32[]{:S(2)}, u32[]{:S(2)}) async-start(bf16[128,6,2048]{2,1,0:T(8,128)(2,1)} %reshape.556), calls=%async_computation | async-start | bytes 8388608 | tf_op jit(solution)/shard_map/all_to_all | solution.py:169
  60.6 1.9 pad_maximum_fusion
  66.6 118.6 %all-to-all-done = bf16[128,6,2048]{2,1,0:T(8,128)(2,1)} async-done(((bf16[128,6,2048]{2,1,0:T(8,128)(2,1)}), bf16[128,6,2048]{2,1,0:T(8,128)(2,1)}, u32[]{:S(2)}, u32[]{:S(2)}) %all-to-all-start) | async-done | bytes 3145760 | tf_op jit(solution)/shard_map/all_to_all | solution.py:169
  185.2 6.5 %reshape.557 = bf16[768,2048]{1,0:T(8,128)(2,1)} reshape(bf16[128,6,2048]{2,1,0:T(8,128)(2,1)} %all-to-all-done) | data formatting | bytes 6291456 | tf_op jit(solution)/shard_map/reshape | solution.py:171
  191.7 5.6 %fusion.34 = f32[768,512]{1,0:T(8,128)} fusion(bf16[768,2048]{1,0:T(8,128)(2,1)} %reshape.557, bf16[1,2048,512]{2,1,0:T(8,128)(2,1)} %param.28), kind=kOutput, calls=%fused_computation.47 | convolution fusion | flops 1610612736 | bytes 6815744 | tf_op jit(solution)/shard_map/dot_general | solution.py:173
  197.3 8.2 %convolution_convert_fusion = bf16[768,2048]{1,0:T(8,128)(2,1)} fusion(bf16[1,512,2048]{2,1,0:T(8,128)(2,1)S(1)} %copy-done, f32[768,512]{1,0:T(8,128)} %fusion.34, bf16[768,2048]{1,0:T(8,128)(2,1)} %reshape.557, bf16[1,2048,512]{2,1,0:T(8,128)(2,1)} %param.29), kind=kOutput, calls=%fused_computation.36 | convolution fusion | flops 3225157632 | bytes 12058624 | tf_op jit(solution)/shard_map/dot_general | solution.py:177
  205.5 6.3 %reshape.558 = bf16[128,6,2048]{2,1,0:T(8,128)(2,1)} reshape(bf16[768,2048]{1,0:T(8,128)(2,1)} %convolution_convert_fusion) | data formatting | bytes 6291456 | tf_op jit(solution)/shard_map/reshape | solution.py:179
  211.7 12.2 %all-to-all-start.1 = ((bf16[128,6,2048]{2,1,0:T(8,128)(2,1)}), bf16[128,6,2048]{2,1,0:T(8,128)(2,1)}, u32[]{:S(2)}, u32[]{:S(2)}) async-start(bf16[128,6,2048]{2,1,0:T(8,128)(2,1)} %reshape.558), calls=%async_computation.1 | async-start | bytes 8388608 | tf_op jit(solution)/shard_map/all_to_all | solution.py:176
  224.0 3.6 fusion.58
  228.3 3.6 collective-permute-start
  231.9 2.3 collective-permute-start.1
  234.3 2.2 collective-permute-done
  236.4 18.4 %collective-permute-done.1 = bf16[128,128]{0,1:T(8,128)(2,1)S(1)} collective-permute-done((bf16[128,128]{0,1:T(8,128)(2,1)S(1)}, bf16[128,128]{0,1:T(8,128)(2,1)S(1)}, u32[]{:S(2)}, u32[]{:S(2)}) %collective-permute-start.1) | collective-permute-done | bytes 32800 | tf_op jit(solution)/shard_map/ppermute | solution.py:34
  254.9 10.4 %while.13 = (s32[]{:T(128)}, bf16[2,512,128]{2,1,0:T(8,128)(2,1)S(1)}, s32[2]{0:T(128)S(1)}, bf16[1280,1,64]{0,2,1:T(8,128)(2,1)S(1)}, s32[]{:T(128)}, /*index=5...) while((s32[]{:T(128)}, ...), condition=%wide.region_4.5_spmd.clone, body=%wide.region_1.4_spmd.clone.sunk | while | flops 212800256 | bytes 12050712 | solution.py:97
  265.3 2.5 fusion.29
  267.8 63.7 %all-to-all-done.1 = bf16[128,6,2048]{2,1,0:T(8,128)(2,1)} async-done(((bf16[128,6,2048]{2,1,0:T(8,128)(2,1)}), bf16[128,6,2048]{2,1,0:T(8,128)(2,1)}, u32[]{:S(2)}, u32[]{:S(2)}) %all-to-all-start.1) | async-done | bytes 3145760 | tf_op jit(solution)/shard_map/all_to_all | solution.py:176
  331.5 4.9 %reshape.559 = bf16[768,2048]{1,0:T(8,128)(2,1)S(1)} reshape(bf16[128,6,2048]{2,1,0:T(8,128)(2,1)} %all-to-all-done.1) | data formatting | bytes 6291456 | tf_op jit(solution)/shard_map/reshape | solution.py:185
  336.4 3.3 gather_fusion
  339.7 4.7 %reshape.560 = f32[128,4,2048]{2,1,0:T(4,128)} reshape(bf16[512,2048]{1,0:T(8,128)(2,1)} %gather_fusion) | data formatting | bytes 6291456 | tf_op jit(solution)/shard_map/convert_element_type | solution.py:186
  344.5 5.5 %multiply_reduce_fusion = f32[128,2048]{1,0:T(8,128)S(1)} fusion(f32[128,4,2048]{2,1,0:T(4,128)} %reshape.560, f32[128,4]{1,0:T(8,128)S(1)} %copy.42), kind=kLoop, calls=%fused_computation.35 | loop fusion | flops 1835008 | bytes 5244928 | tf_op jit(solution)/shard_map/reduce_sum | solution.py:186
  350.0 4.4 %fusion.25 = bf16[128,2048]{1,0:T(8,128)(2,1)} fusion(f32[128,2048]{1,0:T(8,128)S(1)} %multiply_reduce_fusion, bf16[512,6144]{1,0:T(8,128)(2,1)} %all-gather.5.cloned.1.call-done, bf16[128,2048]{1,0:T(8,128)(2,1)} %copy-done.3, f32[128,512]{1,0:T(8,128)S(1)} %fusion.29), kind=kOutput, calls=%fused_computation.38 | convolution fusion | flops 537788416 | bytes 6553600 | tf_op jit(solution)/shard_map/dot_general | solution.py:136
  (101 shorter events, 17.5 us)
Async XLA Ops:
  7.2 190.1 %copy-start = (bf16[1,512,2048]{2,1,0:T(8,128)(2,1)S(1)}, bf16[1,512,2048]{2,1,0:T(8,128)(2,1)}, u32[]{:S(2)}) copy-start(bf16[1,512,2048]{2,1,0:T(8,128)(2,1)} %param.30) | copy-start | bytes 6291460
  7.2 5.1 %copy-start.9 = (s32[128,4]{0,1:T(4,128)S(1)}, s32[128,4]{0,1:T(4,128)}, u32[]{:S(2)}) copy-start(s32[128,4]{0,1:T(4,128)} %param.27) | copy-start | bytes 6148
  7.2 5.5 %copy-start.2 = (bf16[128,2048]{1,0:T(8,128)(2,1)S(1)}, bf16[128,2048]{1,0:T(8,128)(2,1)}, u32[]{:S(2)}) copy-start(bf16[128,2048]{1,0:T(8,128)(2,1)} %param.24) | copy-start | bytes 1572868
  7.2 5.8 %copy-start.10 = (f32[2048]{0:T(1024)S(1)}, f32[2048]{0:T(1024)}, u32[]{:S(2)}) copy-start(f32[2048]{0:T(1024)} %param.25) | copy-start | bytes 24580
  7.2 216.8 %all-gather.3.cloned.1.call-start = ((), (), s32[]{:S(2)}) async-start(), calls=%async_computation.2 | async-start | bytes 4718592 | tf_op jit(solution)/shard_map/all_gather | solution.py:125
  13.2 18.8 %copy-start.3 = (bf16[128,2048]{1,0:T(8,128)(2,1)}, bf16[128,2048]{1,0:T(8,128)(2,1)S(1)}, u32[]{:S(2)}) copy-start(bf16[128,2048]{1,0:T(8,128)(2,1)S(1)} %fusion.57) | copy-start | bytes 1572868
  32.0 28.6 %copy-start.6 = (bf16[64,2048]{1,0:T(8,128)(2,1)S(1)}, bf16[64,2048]{1,0:T(8,128)(2,1)}, u32[]{:S(2)}) copy-start(bf16[64,2048]{1,0:T(8,128)(2,1)} %param.33) | copy-start | bytes 786436
  32.0 28.6 %copy-start.7 = (bf16[2048,64]{0,1:T(8,128)(2,1)S(1)}, bf16[2048,64]{0,1:T(8,128)(2,1)}, u32[]{:S(2)}) copy-start(bf16[2048,64]{0,1:T(8,128)(2,1)} %param.32) | copy-start | bytes 786436
  32.0 30.5 %copy-start.5 = (bf16[2048,64]{0,1:T(8,128)(2,1)S(1)}, bf16[2048,64]{0,1:T(8,128)(2,1)}, u32[]{:S(2)}) copy-start(bf16[2048,64]{0,1:T(8,128)(2,1)} %param.21) | copy-start | bytes 786436
  32.0 153.2 %all-to-all-start = ((bf16[128,6,2048]{2,1,0:T(8,128)(2,1)}), bf16[128,6,2048]{2,1,0:T(8,128)(2,1)}, u32[]{:S(2)}, u32[]{:S(2)}) async-start(bf16[128,6,2048]{2,1,0:T(8,128)(2,1)} %reshape.556), calls=%async_computation | async-start | bytes 8388608 | tf_op jit(solution)/shard_map/all_to_all | solution.py:169
  60.5 204.8 %all-gather.5.cloned.1.call-start = ((), (), s32[]{:S(2)}) async-start(), calls=%async_computation.3 | async-start | bytes 7077888 | tf_op jit(solution)/shard_map/all_gather | solution.py:18
  211.7 12.3 %copy-start.11 = (bf16[2048,128]{1,0:T(8,128)(2,1)S(1)}, bf16[2048,128]{1,0:T(8,128)(2,1)}, u32[]{:S(2)}) copy-start(bf16[2048,128]{1,0:T(8,128)(2,1)} %param.20) | copy-start | bytes 1572868
  211.7 119.8 %all-to-all-start.1 = ((bf16[128,6,2048]{2,1,0:T(8,128)(2,1)}), bf16[128,6,2048]{2,1,0:T(8,128)(2,1)}, u32[]{:S(2)}, u32[]{:S(2)}) async-start(bf16[128,6,2048]{2,1,0:T(8,128)(2,1)} %reshape.558), calls=%async_computation.1 | async-start | bytes 8388608 | tf_op jit(solution)/shard_map/all_to_all | solution.py:176
  227.6 27.3 %copy-start.8 = (f32[2]{0:T(128)S(1)}, f32[2]{0:T(128)}, u32[]{:S(2)}) copy-start(f32[2]{0:T(128)} %param.23) | copy-start | bytes 28
  227.6 27.3 %copy-start.12 = (bf16[2,512,128]{2,1,0:T(8,128)(2,1)S(1)}, bf16[2,512,128]{2,1,0:T(8,128)(2,1)}, u32[]{:S(2)}) copy-start(bf16[2,512,128]{2,1,0:T(8,128)(2,1)} %custom-call.4) | copy-start | bytes 786436
  228.3 8.1 %collective-permute-start = (bf16[128,128]{0,1:T(8,128)(2,1)S(1)}, bf16[128,128]{0,1:T(8,128)(2,1)S(1)}, u32[]{:S(2)}, u32[]{:S(2)}) collective-permute-start(bf16[128,128]{0,1:T(8,128)(2,1)S(1)} %get-tuple-element.175), channel_id=1, source_target_pairs={{0,8},{8,16},{16,24},{24,32},{32,40},{40,48},{48,56},{56,64},{64,7... | collective-permute-start | bytes 98312 | tf_op jit(solution)/shard_map/ppermute | solution.py:31
  231.9 22.9 %collective-permute-start.1 = (bf16[128,128]{0,1:T(8,128)(2,1)S(1)}, bf16[128,128]{0,1:T(8,128)(2,1)S(1)}, u32[]{:S(2)}, u32[]{:S(2)}) collective-permute-start(bf16[128,128]{0,1:T(8,128)(2,1)S(1)} %get-tuple-element.176), channel_id=1, source_target_pairs={{8,0},{16,8},{24,16},{32,24},{40,32},{48,40},{56,48},{64,56},{72,6... | collective-permute-start | bytes 98312 | tf_op jit(solution)/shard_map/ppermute | solution.py:34
  254.9 10.4 %copy-start.4 = (bf16[128,2048]{1,0:T(8,128)(2,1)S(1)}, bf16[128,2048]{1,0:T(8,128)(2,1)}, u32[]{:S(2)}) copy-start(bf16[128,2048]{1,0:T(8,128)(2,1)} %copy-done.3) | copy-start | bytes 1572868
  265.3 2.5 copy-start.13
  344.5 9.9 %copy-start.1 = (bf16[1,512,2048]{2,1,0:T(8,128)(2,1)S(1)}, bf16[1,512,2048]{2,1,0:T(8,128)(2,1)}, u32[]{:S(2)}) copy-start(bf16[1,512,2048]{2,1,0:T(8,128)(2,1)} %param.30) | copy-start | bytes 6291460
Sparse Core Ops, SparseCore 0:
  10.9 130.6 all-gather.2
  143.4 111.8 all-gather.4
where the time goes:
time: 369 us; the launch traced here: 362 us
  waiting for transfers between devices  203 us (55%)
  local copies, waits for them, and re-layouts  49.1 us (13%)
  starting transfers between devices  46.6 us (13%)
  matrix products  29.5 us (8%)
  other arithmetic  16.7 us (5%)
  between operations  15 us (4%)
    all_to_all x1, waiting for transfers between devices, body(): lax.all_to_all(outgoing, ('ep', 'tp'), split_axis=0, concat_axis=0, tiled...  119 us
    all_to_all x1, waiting for transfers between devices, body(): lax.all_to_all(jnp.dot(hidden_rows, expert_down[0], preferred_element_typ...  63.7 us
    all_to_all x1, starting transfers between devices, body(): lax.all_to_all(outgoing, ('ep', 'tp'), split_axis=0, concat_axis=0, tiled...  28.5 us
    ppermute x1, waiting for transfers between devices, extended(): lax.ppermute(lax.slice_in_dim(block, 0, width, axis=dim), axis, backward)  18.4 us
    scatter x1, local copies, waits for them, and re-layouts, body(): outgoing = jnp.zeros((experts * capacity, normed_second.shape[1]), jnp.bf...  12.6 us
    all_to_all x1, starting transfers between devices, body(): lax.all_to_all(jnp.dot(hidden_rows, expert_down[0], preferred_element_typ...  12.2 us
    dot_general x1, matrix products, body(): jnp.dot(hidden_rows, expert_down[0], preferred_element_type=jnp.float32)  8.15 us
  transfers between devices with their start and end apart: 6, of which 4 were waited for; matrix products, arithmetic and copies ran while one was open for 19% of the time, Pallas kernels for 0%

commit v1 on v0

--- a/solution.py
+++ b/solution.py
@@ -1,6 +1,8 @@
 import jax
 import jax.numpy as jnp
 from jax import lax
+from jax.experimental import pallas as pl
+from jax.experimental.pallas import tpu as pltpu
 from jax.sharding import PartitionSpec as P
 
 HEAD_DIM = 64
@@ -10,17 +12,6 @@
 EPS = 1e-06
 THETA = 10000.0
 ROUTED_SCALE = 2.5
-
-
-def turned_gather(arrays, axis, dims):
-    turned = [jnp.moveaxis(a, dim, 0) for a, dim in zip(arrays, dims)]
-    both = jnp.concatenate([t.reshape(len(t), -1) for t in turned], axis=1)
-    whole, at, done = (lax.all_gather(both, axis, axis=0, tiled=True), 0, [])
-    for t, dim in zip(turned, dims):
-        piece = whole[:, at : at + t[0].size].reshape(-1, *t.shape[1:])
-        done.append(jnp.moveaxis(piece, 0, dim))
-        at += t[0].size
-    return tuple(done)
 
 
 def extended(block, sides, width):
@@ -96,6 +87,81 @@
 
     blocks_out = lax.map(one_block, jnp.arange(span_rows // block_rows, dtype=jnp.int32))
     return blocks_out.reshape(span_rows, head_count * head_width)
+
+
+CAP = 6
+FOLD = 4
+TILE = CAP * FOLD
+
+
+def reorder(cells, inverse):
+    size = cells * TILE
+    row = lax.broadcasted_iota(jnp.int32, (size, size), 1 if inverse else 0)
+    col = lax.broadcasted_iota(jnp.int32, (size, size), 0 if inverse else 1)
+    fold = row // (cells * CAP)
+    within = row - fold * (cells * CAP)
+    cell = within // CAP
+    wanted = cell * TILE + fold * CAP + (within - cell * CAP)
+    return (wanted == col).astype(jnp.bfloat16)
+
+
+CELLS = 16
+
+
+def expert_kernel(rows_ref, gate_ref, up_ref, down_ref, into_ref, outof_ref, out_ref):
+    f32, bf16 = jnp.float32, jnp.bfloat16
+    size = CELLS * TILE
+    pieces = rows_ref.shape[0] // size
+    quarter = rows_ref.shape[1]
+    flat = []
+    for piece in range(pieces):
+        block = jnp.dot(
+            into_ref[...], rows_ref[piece * size : (piece + 1) * size], preferred_element_type=f32
+        ).astype(bf16)
+        flat.append(
+            jnp.concatenate(
+                [block[f * CELLS * CAP : (f + 1) * CELLS * CAP] for f in range(FOLD)], axis=1
+            )
+        )
+    tokens = jnp.concatenate(flat, axis=0)
+    gate = jnp.dot(tokens, gate_ref[...], preferred_element_type=f32)
+    up = jnp.dot(tokens, up_ref[...], preferred_element_type=f32)
+    hidden = (gate * (1.0 / (1.0 + jnp.exp(-gate))) * up).astype(bf16)
+    result = jnp.dot(hidden, down_ref[...], preferred_element_type=f32).astype(bf16)
+    for piece in range(pieces):
+        part = result[piece * CELLS * CAP : (piece + 1) * CELLS * CAP]
+        block = jnp.concatenate(
+            [part[:, f * quarter : (f + 1) * quarter] for f in range(FOLD)], axis=0
+        )
+        out_ref[piece * size : (piece + 1) * size] = jnp.dot(
+            outof_ref[...], block, preferred_element_type=f32
+        ).astype(bf16)
+
+
+def run_expert(rows, gate, up, down):
+    height, quarter = rows.shape
+    steps = 4
+    block = height // steps
+    size = CELLS * TILE
+    fixed = lambda i: (0, 0)
+    return pl.pallas_call(
+        expert_kernel,
+        grid=(steps,),
+        in_specs=[
+            pl.BlockSpec((block, quarter), lambda i: (i, 0)),
+            pl.BlockSpec(gate.shape, fixed),
+            pl.BlockSpec(up.shape, fixed),
+            pl.BlockSpec(down.shape, fixed),
+            pl.BlockSpec((size, size), fixed),
+            pl.BlockSpec((size, size), fixed),
+        ],
+        out_specs=pl.BlockSpec((block, quarter), lambda i: (i, 0)),
+        out_shape=jax.ShapeDtypeStruct(rows.shape, rows.dtype),
+        compiler_params=pltpu.CompilerParams(
+            dimension_semantics=("arbitrary",), vmem_limit_bytes=48 * 1024 * 1024
+        ),
+        name="expert",
+    )(rows, gate, up, down, reorder(CELLS, False), reorder(CELLS, True))
 
 
 def body(
@@ -116,8 +182,79 @@
     shared_up,
     shared_down,
 ):
+    f32, bf16 = jnp.float32, jnp.bfloat16
+    columns, rows = lax.axis_size("tp"), lax.axis_size("ep")
     normed_first = rms_rows(mixer_in, mixer_gain)
     normed_second = rms_rows(moe_in, moe_gain)
+    tokens, width = normed_second.shape
+    experts = router.shape[1]
+    quarter = width // FOLD
+
+    named = routes.T
+    hit = jnp.any(named[None] == jnp.arange(experts, dtype=jnp.int32)[:, None, None], axis=1)
+    earlier = (jnp.arange(tokens)[:, None] < jnp.arange(tokens)[None, :]).astype(bf16)
+    rank = jnp.dot(hit.astype(bf16), earlier, preferred_element_type=f32)
+    code = jnp.where(hit, rank, -1.0)
+    place = jnp.arange(TILE, dtype=jnp.int32)
+    lane = jnp.arange(FOLD * tokens, dtype=jnp.int32)
+    same_fold = (place[:, None] // CAP) == (lane[None, :] // tokens)
+    picks = (jnp.tile(code, (1, FOLD))[:, None, :] == (place % CAP).astype(f32)[None, :, None]) & same_fold[None]
+    stacked_rows = jnp.concatenate(
+        [normed_second[:, f * quarter : (f + 1) * quarter] for f in range(FOLD)], axis=0
+    )
+    outgoing = jnp.dot(
+        picks.astype(bf16).reshape(experts * TILE, FOLD * tokens),
+        stacked_rows,
+        preferred_element_type=f32,
+    ).astype(bf16)
+    arrived = lax.all_to_all(
+        outgoing.reshape(experts, TILE, quarter), ("ep", "tp"), split_axis=0, concat_axis=0, tiled=True
+    )
+    results = run_expert(
+        arrived.reshape(experts * TILE, quarter), expert_gate[0], expert_up[0], expert_down[0]
+    )
+    returned = lax.all_to_all(
+        results.reshape(experts, TILE, quarter), ("ep", "tp"), split_axis=0, concat_axis=0, tiled=True
+    ).reshape(experts * TILE, quarter)
+
+    affinity = jax.nn.sigmoid(
+        lax.dot_general(router, normed_second, (((0,), (1,)), ((), ())), preferred_element_type=f32)
+    )
+    chosen = jnp.where(hit, affinity, 0.0)
+    weight = ROUTED_SCALE * chosen / jnp.sum(chosen, axis=0, keepdims=True)
+    coarse = lax.reduce_precision(weight, 8, 7)
+
+    def mixing(scale):
+        spread = jnp.tile(scale.astype(bf16), (1, FOLD))[:, None, :]
+        return jnp.where(picks, spread, 0.0).reshape(experts * TILE, FOLD * tokens)
+
+    def mixed_by(scale):
+        return lax.dot_general(
+            mixing(scale), returned, (((0,), (0,)), ((), ())), preferred_element_type=f32
+        )
+
+    routed = mixed_by(coarse) + mixed_by(weight - coarse)
+    routed = jnp.concatenate([routed[f * tokens : (f + 1) * tokens] for f in range(FOLD)], axis=1)
+
+    part = width // rows
+    start = lax.axis_index("ep") * part
+    piece = jnp.concatenate(
+        [
+            lax.dynamic_slice_in_dim(jnp.concatenate([shared_gate, shared_up], axis=1), start, part, 0),
+            lax.dynamic_slice_in_dim(shared_down, start, part, 1),
+        ],
+        axis=0,
+    )
+    units = shared_gate.shape[1]
+    whole = lax.all_gather(piece, ("ep", "tp"), axis=0, tiled=False)
+    whole = whole.reshape(rows, columns, part + units, part)
+    both = jnp.transpose(whole[:, :, :part], (0, 2, 1, 3)).reshape(width, columns * 2 * units)
+    full_down = jnp.transpose(whole[:, :, part:], (1, 2, 0, 3)).reshape(columns * units, width)
+    lifted = jnp.dot(normed_second, both, preferred_element_type=f32).reshape(tokens, columns, 2 * units)
+    hidden = (jax.nn.silu(lifted[..., :units]) * lifted[..., units:]).astype(bf16)
+    shared = jnp.dot(hidden.reshape(tokens, columns * units), full_down, preferred_element_type=f32)
+    moe_out = (routed + shared).astype(bf16)
+
     query_cols = w_query.shape[1]
     key_cols = w_key.shape[1]
     joined = jnp.concatenate([w_query, w_key, w_value], axis=1)
@@ -126,14 +263,6 @@
         joined,
         preferred_element_type=jnp.float32,
     )
-    full_gate, full_up, full_down = turned_gather(
-        (shared_gate, shared_up, shared_down), "tp", (1, 1, 0)
-    )
-    hidden = (
-        jax.nn.silu(jnp.dot(normed_second, full_gate, preferred_element_type=jnp.float32))
-        * jnp.dot(normed_second, full_up, preferred_element_type=jnp.float32)
-    ).astype(jnp.bfloat16)
-    shared = jnp.dot(hidden, full_down, preferred_element_type=jnp.float32)
     span_rows = projected.shape[0]
     offset = lax.axis_index("ep") * span_rows
     seq_length = span_rows * lax.axis_size("ep")
@@ -148,43 +277,6 @@
     stacked = jnp.concatenate([key_rows.reshape(span_rows, key_cols), value_rows], axis=1)
     padded = extended(stacked, (("ep", 0),), WINDOW)
     mixed = attend(query_rows, padded, sink_logit, offset, seq_length)
-    tokens = normed_second.shape[0]
-    top_count = routes.shape[1]
-    experts = router.shape[1]
-    capacity = 3 * top_count * tokens // (2 * experts)
-    affinity = jax.nn.sigmoid(jnp.dot(normed_second, router, preferred_element_type=jnp.float32))
-    hit_table = routes[:, :, None] == jnp.arange(experts, dtype=jnp.int32)[None, None, :]
-    chosen = jnp.sum(jnp.where(hit_table, affinity[:, None, :], 0.0), axis=-1)
-    route_weight = ROUTED_SCALE * chosen / jnp.sum(chosen, axis=-1, keepdims=True)
-    flat_hits = hit_table.reshape(tokens * top_count, experts).astype(jnp.int32)
-    slot_index = jnp.sum((jnp.cumsum(flat_hits, axis=0) - 1) * flat_hits, axis=-1)
-    target = routes.reshape(-1) * capacity + slot_index
-    source = jnp.arange(tokens * top_count, dtype=jnp.int32) // top_count
-    outgoing = (
-        jnp.zeros((experts * capacity, normed_second.shape[1]), jnp.bfloat16)
-        .at[target]
-        .set(normed_second[source])
-    )
-    outgoing = outgoing.reshape(experts, capacity, -1)
-    row_block = lax.all_to_all(outgoing, ("ep", "tp"), split_axis=0, concat_axis=0, tiled=True)
-    row_shape = row_block.shape
-    flat_rows = row_block.reshape(-1, row_shape[-1])
-    hidden_rows = (
-        jax.nn.silu(jnp.dot(flat_rows, expert_gate[0], preferred_element_type=jnp.float32))
-        * jnp.dot(flat_rows, expert_up[0], preferred_element_type=jnp.float32)
-    ).astype(jnp.bfloat16)
-    returned = lax.all_to_all(
-        jnp.dot(hidden_rows, expert_down[0], preferred_element_type=jnp.float32)
-        .astype(jnp.bfloat16)
-        .reshape(row_shape),
-        ("ep", "tp"),
-        split_axis=0,
-        concat_axis=0,
-        tiled=True,
-    )
-    picked = returned.reshape(experts * capacity, -1)[target].reshape(tokens, top_count, -1)
-    routed = jnp.sum(picked.astype(jnp.float32) * route_weight[:, :, None], axis=1)
-    moe_out = (routed + shared).astype(jnp.bfloat16)
     return (mixed, moe_out)
 
 

time: 369 us -> 332 us (0.90); the launches traced: 362 us -> 331 us
  waiting for transfers between devices: 203 us -> 186 us
  local copies, waits for them, and re-layouts: 49.1 us -> 33.9 us
  Pallas kernels: 0 us -> 12 us
  matrix products: 29.5 us -> 24.9 us
    all_to_all x2, waiting for transfers between devices: 182 us -> 95.8 us  [the longest x1 95.8 us: body(): lax.all_to_all(outgoing.reshape(experts, TILE, quarter), ('ep', 'tp'), sp...]
    all_gather x1, waiting for transfers between devices: 0.02 us -> 32.8 us  [body(): whole = lax.all_gather(piece, ('ep', 'tp'), axis=0, tiled=False)]
    ppermute x1, waiting for transfers between devices: 18.4 us -> 49.4 us  [extended(): lax.ppermute(lax.slice_in_dim(block, 0, width, axis=dim), axis, backward)]
    reshape x4 -> x0, local copies, waits for them, and re-layouts: 23.9 us -> none  [the longest x1 6.53 us: body(): flat_rows = row_block.reshape(-1, row_shape[-1])]
    scatter x1 -> x0, local copies, waits for them, and re-layouts: 12.6 us -> none  [body(): outgoing = jnp.zeros((experts * capacity, normed_second.shape[1]), jnp.bf...]
    pallas_call x0 -> x1, Pallas kernels: none -> 12 us  [run_expert(): pl.pallas_call(expert_kernel, grid=(steps,), in_specs=[pl.BlockSpec((bloc...]
    transpose x0 -> x4, local copies, waits for them, and re-layouts: none -> 11.7 us  [the longest x2 8.45 us: body(): jnp.transpose(whole[:, :, :part], (0, 2, 1, 3))]
    unnamed x31 -> x59, local copies, waits for them, and re-layouts: 2.37 us -> 12.2 us
  transfers between devices with their start and end apart: 6 -> 6, of which waited for: 4 -> 4; matrix products, arithmetic and copies ran while one was open for 19% -> 11% of each run, Pallas kernels for 0% -> 4%
where the time goes in v1:
time: 332 us; the launch traced here: 331 us
  waiting for transfers between devices  186 us (56%)
  starting transfers between devices  45.6 us (14%)
  local copies, waits for them, and re-layouts  33.9 us (10%)
  matrix products  24.9 us (8%)
  between operations  14.7 us (4%)
  other arithmetic  13.2 us (4%)
  Pallas kernels  12 us (4%)
    all_to_all x1, waiting for transfers between devices, body(): lax.all_to_all(outgoing.reshape(experts, TILE, quarter), ('ep', 'tp'), sp...  95.8 us
    ppermute x1, waiting for transfers between devices, extended(): lax.ppermute(lax.slice_in_dim(block, 0, width, axis=dim), axis, backward)  49.4 us
    all_gather x1, waiting for transfers between devices, body(): whole = lax.all_gather(piece, ('ep', 'tp'), axis=0, tiled=False)  32.8 us
    all_to_all x1, starting transfers between devices, body(): lax.all_to_all(outgoing.reshape(experts, TILE, quarter), ('ep', 'tp'), sp...  28.4 us
    unnamed x59, local copies, waits for them, and re-layouts  12.2 us
    pallas_call x1, Pallas kernels, run_expert(): pl.pallas_call(expert_kernel, grid=(steps,), in_specs=[pl.BlockSpec((bloc...  12 us
    all_to_all x1, starting transfers between devices, body(): lax.all_to_all(results.reshape(experts, TILE, quarter), ('ep', 'tp'), spl...  11 us
    dot_general x2, matrix products, mixed_by(): lax.dot_general(mixing(scale), returned, (((0,), (0,)), ((), ())), prefer...  9.02 us
  transfers between devices with their start and end apart: 6, of which 4 were waited for; matrix products, arithmetic and copies ran while one was open for 11% of the time, Pallas kernels for 4%

profile of v1, /device:TPU:513, one launch (start us, length us, event | category | flops | bytes accessed | tf_op | source)
XLA Modules:
  0.0 331.4 jit_solution(15676465047113229934)
XLA Ops:
  8.6 2.0 fusion.61
  13.4 3.4 %convolution_convert_fusion = bf16[3072,512]{1,0:T(8,128)(2,1)} fusion(pred[3072,512]{1,0:T(32,128)(4,1)S(1)} %fusion.25, bf16[128,512]{1,0:T(8,128)(2,1)S(1)} %get-tuple-element.182, bf16[128,512]{1,0:T(8,128)(2,1)S(1)} %get-tuple-element.183, bf16[128,512]{1,0:T(8,128)(2,1)S(1)} %get-tuple-element.184, bf16[128,512]{1,0:T(8,128)(2,1)S(1)} %get-tuple-element.181), kind=kOutput, calls=%fused_computation.37 | convolution fusion | flops 1614282752 | bytes 5242880 | tf_op jit(solution)/shard_map/dot_general | solution.py:205
  16.9 28.4 %all-to-all-start = ((bf16[128,24,512]{2,1,0:T(8,128)(2,1)}), bf16[128,24,512]{2,1,0:T(8,128)(2,1)}, u32[]{:S(2)}, u32[]{:S(2)}) async-start(bf16[128,24,512]{2,1,0:T(8,128)(2,1)} %bitcast.158), calls=%async_computation | async-start | bytes 6291456 | tf_op jit(solution)/shard_map/all_to_all | solution.py:210
  52.6 2.0 copy.52
  56.5 95.8 %all-to-all-done = bf16[128,24,512]{2,1,0:T(8,128)(2,1)} async-done(((bf16[128,24,512]{2,1,0:T(8,128)(2,1)}), bf16[128,24,512]{2,1,0:T(8,128)(2,1)}, u32[]{:S(2)}, u32[]{:S(2)}) %all-to-all-start) | async-done | bytes 3145760 | tf_op jit(solution)/shard_map/all_to_all | solution.py:210
  152.3 1.6 copy-done.3
  153.9 12.0 %expert.1 = bf16[3072,512]{1,0:T(8,128)(2,1)} custom-call(bf16[3072,512]{1,0:T(8,128)(2,1)} %bitcast.15.rows_ref, bf16[2048,512]{1,0:T(8,128)(2,1)S(1)} %bitcast.149, bf16[2048,512]{1,0:T(8,128)(2,1)S(1)} %bitcast.150, bf16[512,2048]{1,0:T(8,128)(2,1)} %bitcast.159, bf16[384,384]{1,0:T(8,128)(2,1)S(1)} %get-tuple-element.194.into_ref, ...), custom_call_target="tpu_custom_call" | custom-call | tf_op jit(solution)/shard_map/expert/pallas_call | solution.py:147
  165.9 11.0 %all-to-all-start.1 = ((bf16[128,24,512]{2,1,0:T(8,128)(2,1)}), bf16[128,24,512]{2,1,0:T(8,128)(2,1)}, u32[]{:S(2)}, u32[]{:S(2)}) async-start(bf16[128,24,512]{2,1,0:T(8,128)(2,1)} %bitcast.154), calls=%async_computation.1 | async-start | bytes 6291456 | tf_op jit(solution)/shard_map/all_to_all | solution.py:216
  177.0 3.6 %fusion.65 = f32[1024,256]{0,1:T(8,128)S(1)} fusion(bf16[1024,2048]{1,0:T(8,128)(2,1)} %all-gather.4.cloned.1.call-done, bf16[2048,64]{1,0:T(8,128)(2,1)S(1)} %copy-done.9, bf16[2048,64]{1,0:T(8,128)(2,1)S(1)} %copy-done.8, bf16[2048,128]{1,0:T(8,128)(2,1)S(1)} %copy-done.22), kind=kOutput, calls=%fused_computation.77 | convolution fusion | flops 1076887552 | bytes 6291456 | tf_op jit(solution)/shard_map/dot_general | solution.py:261
  181.3 3.7 %collective-permute-start = (bf16[128,128]{0,1:T(8,128)(2,1)S(1)}, bf16[128,128]{0,1:T(8,128)(2,1)S(1)}, u32[]{:S(2)}, u32[]{:S(2)}) collective-permute-start(bf16[128,128]{0,1:T(8,128)(2,1)S(1)} %get-tuple-element.189), channel_id=1, source_target_pairs={{0,8},{8,16},{16,24},{24,32},{32,40},{40,48},{48,56},{56,64},{64,7... | collective-permute-start | bytes 98312 | tf_op jit(solution)/shard_map/ppermute | solution.py:22
  185.0 2.3 collective-permute-start.1
  187.4 7.4 %collective-permute-done = bf16[128,128]{0,1:T(8,128)(2,1)S(1)} collective-permute-done((bf16[128,128]{0,1:T(8,128)(2,1)S(1)}, bf16[128,128]{0,1:T(8,128)(2,1)S(1)}, u32[]{:S(2)}, u32[]{:S(2)}) %collective-permute-start) | collective-permute-done | bytes 32800 | tf_op jit(solution)/shard_map/ppermute | solution.py:22
  194.9 49.4 %collective-permute-done.1 = bf16[128,128]{0,1:T(8,128)(2,1)S(1)} collective-permute-done((bf16[128,128]{0,1:T(8,128)(2,1)S(1)}, bf16[128,128]{0,1:T(8,128)(2,1)S(1)}, u32[]{:S(2)}, u32[]{:S(2)}) %collective-permute-start.1) | collective-permute-done | bytes 32800 | tf_op jit(solution)/shard_map/ppermute | solution.py:25
  244.4 10.4 %while.13 = (s32[]{:T(128)}, bf16[2,512,128]{2,1,0:T(8,128)(2,1)S(1)}, s32[2]{0:T(128)S(1)}, bf16[1280,1,64]{0,2,1:T(8,128)(2,1)S(1)}, s32[]{:T(128)}, /*index=5...) while((s32[]{:T(128)}, ...), condition=%wide.region_4.5_spmd.clone, body=%wide.region_1.4_spmd.clone.sunk | while | flops 212800256 | bytes 12050720 | solution.py:88
  254.7 32.8 %all-gather.6.cloned.1.call-done = bf16[24576,128]{1,0:T(8,128)(2,1)} async-done(((bf16[192,128]{1,0:T(8,128)(2,1)}), bf16[24576,128]{1,0:T(8,128)(2,1)}) %all-gather.6.cloned.1.call-update) | async-done | bytes 6291472 | tf_op jit(solution)/shard_map/all_gather | solution.py:249
  287.6 1.9 slice_bitcast_fusion.1
  289.4 4.9 %slice_bitcast_fusion = bf16[16,128,8,128]{3,1,2,0:T(8,128)(2,1)} fusion(bf16[16,8,192,128]{3,2,1,0:T(8,128)(2,1)} %bitcast.156), kind=kLoop, calls=%fused_computation.39 | loop fusion | bytes 8388608 | tf_op jit(solution)/shard_map/transpose | solution.py:251
  294.4 4.4 %fusion.45 = f32[512,512]{0,1:T(8,128)S(1)} fusion(bf16[128,24,512]{2,1,0:T(8,128)(2,1)} %all-to-all-done.1, f32[128,512]{1,0:T(8,128)S(1)} %bitcast.163, f32[24]{0:T(128)S(1)} %get-tuple-element.200, pred[24,512]{1,0:T(8,128)(4,1)S(1)} %broadcast_compare_fusion.2, bf16[128,512]{1,0:T(8,128)(2,1)S(1)} %bitcast.171), kind=kOutput, calls=%fused_computation.57 | convolution fusion | flops 1615331328 | bytes 4599904 | tf_op jit(solution)/shard_map/dot_general | solution.py:232
  298.9 4.6 %fusion.51 = f32[512,512]{0,1:T(8,128)S(1)} fusion(f32[512,512]{0,1:T(8,128)S(1)} %fusion.45, bf16[128,24,512]{2,1,0:T(8,128)(2,1)} %all-to-all-done.1, f32[128,512]{1,0:T(8,128)S(1)} %bitcast.164, f32[24]{0:T(128)S(1)} %get-tuple-element.200, pred[24,512]{1,0:T(8,128)(4,1)S(1)} %broadcast_compare_fusion.2, bf16[128,512]{1,0:T(8,128)(2,1)S(1)} %bitcast.170), kind=kOutput, calls=%fused_computation.59 | convolution fusion | flops 1615593472 | bytes 5648480 | tf_op jit(solution)/shard_map/dot_general | solution.py:232
  304.3 3.5 %copy.56 = bf16[16,128,8,128]{3,2,1,0:T(8,128)(2,1)S(1)} copy(bf16[16,128,8,128]{3,1,2,0:T(8,128)(2,1)S(1)} %copy-done.4) | data formatting | bytes 8388608 | tf_op jit(solution)/shard_map/transpose | solution.py:251
  307.9 3.1 copy.78
  310.9 6.6 %copy.57 = bf16[1024,2048]{1,0:T(8,128)(2,1)} copy(bf16[1024,2048]{0,1:T(8,128)(2,1)} %bitcast.153) | data formatting | bytes 8388608 | tf_op jit(solution)/shard_map/dot_general | solution.py:253
  317.5 3.4 %fusion.90 = f32[128,8,128]{0,2,1:T(8,128)S(1)} fusion(bf16[8,128,2048]{2,1,0:T(8,128)(2,1)} %bitcast.151, bf16[128,2048]{1,0:T(8,128)(2,1)S(1)} %fusion.64), kind=kOutput, calls=%fused_computation.112 | convolution fusion | flops 536870912 | bytes 5242880 | tf_op jit(solution)/shard_map/dot_general | solution.py:253
  321.1 1.4 copy.58
  (128 shorter events, 25.8 us)
Async XLA Ops:
  7.2 42.6 %copy-start = (bf16[2048,128]{1,0:T(8,128)(2,1)S(1)}, bf16[2048,128]{1,0:T(8,128)(2,1)}, u32[]{:S(2)}) copy-start(bf16[2048,128]{1,0:T(8,128)(2,1)} %param.26) | copy-start | bytes 1572868
  7.2 5.8 %copy-start.5 = (bf16[128,2048]{1,0:T(8,128)(2,1)S(1)}, bf16[128,2048]{1,0:T(8,128)(2,1)}, u32[]{:S(2)}) copy-start(bf16[128,2048]{1,0:T(8,128)(2,1)} %param.24) | copy-start | bytes 1572868
  7.2 6.0 %copy-start.21 = (f32[2048]{0:T(1024)S(1)}, f32[2048]{0:T(1024)}, u32[]{:S(2)}) copy-start(f32[2048]{0:T(1024)} %param.25) | copy-start | bytes 24580
  7.2 169.7 %all-gather.4.cloned.1.call-start = ((), (), s32[]{:S(2)}) async-start(), calls=%async_computation.2 | async-start | bytes 4718592 | tf_op jit(solution)/shard_map/all_gather | solution.py:262
  16.9 28.5 %copy-start.12 = (bf16[2048,64]{0,1:T(8,128)(2,1)S(1)}, bf16[2048,64]{0,1:T(8,128)(2,1)}, u32[]{:S(2)}) copy-start(bf16[2048,64]{0,1:T(8,128)(2,1)} %param.31) | copy-start | bytes 786436
  16.9 29.5 %copy-start.13 = (bf16[2048,64]{0,1:T(8,128)(2,1)S(1)}, bf16[2048,64]{0,1:T(8,128)(2,1)}, u32[]{:S(2)}) copy-start(bf16[2048,64]{0,1:T(8,128)(2,1)} %param.32) | copy-start | bytes 786436
  16.9 135.4 %all-to-all-start = ((bf16[128,24,512]{2,1,0:T(8,128)(2,1)}), bf16[128,24,512]{2,1,0:T(8,128)(2,1)}, u32[]{:S(2)}, u32[]{:S(2)}) async-start(bf16[128,24,512]{2,1,0:T(8,128)(2,1)} %bitcast.158), calls=%async_computation | async-start | bytes 6291456 | tf_op jit(solution)/shard_map/all_to_all | solution.py:210
  45.3 242.3 %all-gather.6.cloned.1.call-start = ((), (), s32[]{:S(2)}) async-start(), calls=%async_computation.3 | async-start | bytes 6340608 | tf_op jit(solution)/shard_map/all_gather | solution.py:249
  46.4 105.9 %copy-start.2 = (bf16[1,2048,512]{2,1,0:T(8,128)(2,1)S(1)}, bf16[1,2048,512]{2,1,0:T(8,128)(2,1)}, u32[]{:S(2)}) copy-start(bf16[1,2048,512]{2,1,0:T(8,128)(2,1)} %param.28) | copy-start | bytes 6291460
  165.9 11.1 %copy-start.8 = (bf16[2048,64]{1,0:T(8,128)(2,1)S(1)}, bf16[2048,64]{1,0:T(8,128)(2,1)}, u32[]{:S(2)}) copy-start(bf16[2048,64]{1,0:T(8,128)(2,1)} %copy.51) | copy-start | bytes 786436
  165.9 11.1 %copy-start.9 = (bf16[2048,64]{1,0:T(8,128)(2,1)S(1)}, bf16[2048,64]{1,0:T(8,128)(2,1)}, u32[]{:S(2)}) copy-start(bf16[2048,64]{1,0:T(8,128)(2,1)} %copy.52) | copy-start | bytes 786436
  165.9 11.1 %copy-start.22 = (bf16[2048,128]{1,0:T(8,128)(2,1)S(1)}, bf16[2048,128]{1,0:T(8,128)(2,1)}, u32[]{:S(2)}) copy-start(bf16[2048,128]{1,0:T(8,128)(2,1)} %param.20) | copy-start | bytes 1572868
  165.9 128.5 %all-to-all-start.1 = ((bf16[128,24,512]{2,1,0:T(8,128)(2,1)}), bf16[128,24,512]{2,1,0:T(8,128)(2,1)}, u32[]{:S(2)}, u32[]{:S(2)}) async-start(bf16[128,24,512]{2,1,0:T(8,128)(2,1)} %bitcast.154), calls=%async_computation.1 | async-start | bytes 6291456 | tf_op jit(solution)/shard_map/all_to_all | solution.py:216
  176.9 10.4 %copy-start.10 = (f32[1024,32]{0,1:T(8,128)S(1)}, f32[1024,32]{0,1:T(8,128)}, u32[]{:S(2)}) copy-start(f32[1024,32]{0,1:T(8,128)} %get-tuple-element.195) | copy-start | bytes 393220
  176.9 10.4 %copy-start.11 = (f32[1024,32]{0,1:T(8,128)S(1)}, f32[1024,32]{0,1:T(8,128)}, u32[]{:S(2)}) copy-start(f32[1024,32]{0,1:T(8,128)} %get-tuple-element.196) | copy-start | bytes 393220
  180.6 63.7 %copy-start.20 = (f32[2]{0:T(128)S(1)}, f32[2]{0:T(128)}, u32[]{:S(2)}) copy-start(f32[2]{0:T(128)} %param.23) | copy-start | bytes 28
  180.6 63.7 %copy-start.23 = (bf16[2,512,128]{2,1,0:T(8,128)(2,1)S(1)}, bf16[2,512,128]{2,1,0:T(8,128)(2,1)}, u32[]{:S(2)}) copy-start(bf16[2,512,128]{2,1,0:T(8,128)(2,1)} %custom-call) | copy-start | bytes 786436
  181.3 13.6 %collective-permute-start = (bf16[128,128]{0,1:T(8,128)(2,1)S(1)}, bf16[128,128]{0,1:T(8,128)(2,1)S(1)}, u32[]{:S(2)}, u32[]{:S(2)}) collective-permute-start(bf16[128,128]{0,1:T(8,128)(2,1)S(1)} %get-tuple-element.189), channel_id=1, source_target_pairs={{0,8},{8,16},{16,24},{24,32},{32,40},{40,48},{48,56},{56,64},{64,7... | collective-permute-start | bytes 98312 | tf_op jit(solution)/shard_map/ppermute | solution.py:22
  185.0 59.2 %collective-permute-start.1 = (bf16[128,128]{0,1:T(8,128)(2,1)S(1)}, bf16[128,128]{0,1:T(8,128)(2,1)S(1)}, u32[]{:S(2)}, u32[]{:S(2)}) collective-permute-start(bf16[128,128]{0,1:T(8,128)(2,1)S(1)} %get-tuple-element.190), channel_id=1, source_target_pairs={{8,0},{16,8},{24,16},{32,24},{40,32},{48,40},{56,48},{64,56},{72,6... | collective-permute-start | bytes 98312 | tf_op jit(solution)/shard_map/ppermute | solution.py:25
  254.7 32.8 %copy-start.24 = (bf16[2,512,128]{2,1,0:T(8,128)(2,1)}, bf16[2,512,128]{2,1,0:T(8,128)(2,1)S(1)}, u32[]{:S(2)}) copy-start(bf16[2,512,128]{2,1,0:T(8,128)(2,1)S(1)} %get-tuple-element.127) | copy-start | bytes 786436
  289.4 4.9 %copy-start.7 = (f32[16,8,4,128]{3,1,2,0:T(8,128)S(1)}, f32[16,8,4,128]{3,1,2,0:T(8,128)}, u32[]{:S(2)}) copy-start(f32[16,8,4,128]{3,1,2,0:T(8,128)} %copy-done.6) | copy-start | bytes 786436
  289.4 4.9 %copy-start.19 = (bf16[16,8,4,128]{3,1,2,0:T(8,128)(2,1)S(1)}, bf16[16,8,4,128]{3,1,2,0:T(8,128)(2,1)}, u32[]{:S(2)}) copy-start(bf16[16,8,4,128]{3,1,2,0:T(8,128)(2,1)} %copy.80) | copy-start | bytes 393220
  294.4 4.5 %copy-start.18 = (bf16[16,8,4,128]{3,1,2,0:T(8,128)(2,1)S(1)}, bf16[16,8,4,128]{3,1,2,0:T(8,128)(2,1)}, u32[]{:S(2)}) copy-start(bf16[16,8,4,128]{3,1,2,0:T(8,128)(2,1)} %copy.81) | copy-start | bytes 393220
  298.8 5.5 %copy-start.4 = (bf16[16,128,8,128]{3,1,2,0:T(8,128)(2,1)S(1)}, bf16[16,128,8,128]{3,1,2,0:T(8,128)(2,1)}, u32[]{:S(2)}) copy-start(bf16[16,128,8,128]{3,1,2,0:T(8,128)(2,1)} %slice_bitcast_fusion) | copy-start | bytes 12582916
  (7 other events, 15.2 us)
Sparse Core Ops, SparseCore 0:
  10.8 141.6 all-gather.3
  155.1 132.4 all-gather.5
